TPU v7x, 128 devices: a whole 4x4x4 slice. The times are simulated.
128 devices in a mesh: rep: 16 (over z, x), fs: 4 (over y), tp: 2 (over core).
Axes of the slice: x: 4, y: 4, z: 4, core: 2. Of those that a mesh axis runs over, the one named last changes fastest.
Arguments:
- inputs: bfloat16 [16384, 2048], P(('rep', 'fs', 'tp')), may hold values from -6 to 6
- out_grad: bfloat16 [16384, 2048], P(('rep', 'fs', 'tp')), may hold values from -24 to 24
- pre_act: bfloat16 [16384, 8192], P('rep', ('fs', 'tp')), may hold values from -6 to 6
- w_up: bfloat16 [2048, 8192], P('rep', ('fs', 'tp')), may hold values from -0.125 to 0.125
- w_down_t: bfloat16 [2048, 8192], P('rep', ('fs', 'tp')), may hold values from -0.0625 to 0.0625
Outputs:
- grad_in: bfloat16 [16384, 2048], P(('rep', 'fs', 'tp'))
- grad_up: float32 [2048, 8192], P('rep', ('fs', 'tp'))
- grad_down_t: float32 [2048, 8192], P('rep', ('fs', 'tp'))
All inputs are finite; a program needn't handle non-finite values.
Results may differ from a plain program's by a relative error of at most 0.014.
Values may be sent and summed in bfloat16 or wider, within the bound.
A program may use at most 128 MiB of HBM per device.

v0:
```python
import jax
import jax.numpy as jnp
from jax import lax
from jax.sharding import PartitionSpec as P


def side_by_side(arrays, axis, dim, along):
    widths = [a.shape[along] for a in arrays]
    both = jnp.concatenate(arrays, axis=along)
    out = lax.all_gather(both, axis, axis=dim, tiled=True)
    return tuple(jnp.split(out, [sum(widths[:k]) for k in range(1, len(widths))], axis=along))


def cut_along(shard, dim, length):
    shape = shard.shape
    tiles = shard.reshape(*shape[:dim], length, shape[dim] // length, *shape[dim + 1 :])
    return jnp.moveaxis(tiles, dim, 0)


def sent_and_summed(shard, axis, dim):
    tiles = cut_along(shard, dim, lax.axis_size(axis))
    arrived = lax.all_to_all(tiles, axis, split_axis=0, concat_axis=0, tiled=True)
    return arrived.astype(jnp.float32).sum(axis=0)


def on_device(inputs, out_grad, pre_act, w_up, w_down_t):
    input_rows, grad_rows = side_by_side((inputs, out_grad), ("fs", "tp"), 0, 1)
    row_count, col_count = pre_act.shape
    pre_float = pre_act.astype(jnp.float32)
    linear = jnp.maximum(pre_float, 0.0)
    squared = (linear * linear).astype(jnp.bfloat16)
    grad_squared = jnp.dot(
        grad_rows,
        lax.all_gather(w_down_t, "rep", axis=0, tiled=True),
        preferred_element_type=jnp.float32,
    )
    grad_pre = (grad_squared * 2.0 * linear).astype(jnp.bfloat16)
    partial_terms = lax.dot_general(
        grad_pre,
        lax.all_gather(w_up, "rep", axis=0, tiled=True),
        (((1,), (1,)), ((), ())),
        preferred_element_type=jnp.float32,
    ).astype(jnp.bfloat16)
    grad_in = sent_and_summed(
        partial_terms.astype(jnp.float32).astype(jnp.bfloat16), ("fs", "tp"), 0
    ).astype(jnp.bfloat16)
    total_tokens = row_count * lax.axis_size("rep")
    factor = float(total_tokens) ** (-0.5)
    down_part = lax.dot_general(
        grad_rows, squared, (((0,), (0,)), ((), ())), preferred_element_type=jnp.float32
    )
    up_part = lax.dot_general(
        input_rows, grad_pre, (((0,), (0,)), ((), ())), preferred_element_type=jnp.float32
    )
    stacked = lax.psum_scatter(
        (jnp.concatenate([down_part, up_part], axis=1) * factor).astype(jnp.bfloat16),
        "rep",
        scatter_dimension=0,
        tiled=True,
    ).astype(jnp.float32)
    grad_down_t = stacked[:, :col_count]
    grad_up = stacked[:, col_count:]
    return (grad_in, grad_up, grad_down_t)


def solution(mesh):
    in_specs = (
        P(("rep", "fs", "tp"), None),
        P(("rep", "fs", "tp"), None),
        P("rep", ("fs", "tp")),
        P("rep", ("fs", "tp")),
        P("rep", ("fs", "tp")),
    )
    out_specs = (P(("rep", "fs", "tp"), None), P("rep", ("fs", "tp")), P("rep", ("fs", "tp")))
    return jax.shard_map(
        on_device, mesh=mesh, in_specs=in_specs, out_specs=out_specs, check_vma=False
    )
```

profile of v0, /device:TPU:0, one launch (start us, length us, event | category | flops | bytes accessed | tf_op | source)
XLA Modules:
  0.0 267.7 jit_solution(14350902395174839867)
XLA Ops:
  7.2 0.0 all-gather.4.cloned.1.call-start
  7.2 2.4 pad_maximum_fusion
  9.6 0.0 all-gather.4.cloned.1.call-update
  9.6 0.0 all-gather.6.cloned.1.call-start
  9.6 0.7 all-gather.6.cloned.1.call-update
  10.3 0.0 all-gather.8.cloned.1.call-start
  10.4 0.7 all-gather.8.cloned.1.call-update
  11.1 0.0 copy-start.1
  11.1 0.0 reduce-scatter.4.cloned.1.call-start
  11.1 50.8 %all-gather.4.cloned.1.call-done = bf16[1024,4096]{1,0:T(8,128)(2,1)} async-done(((bf16[128,4096]{1,0:T(8,128)(2,1)}), bf16[1024,4096]{1,0:T(8,128)(2,1)}) %all-gather.4.cloned.1.call-update) | async-done | bytes 8388624 | tf_op jit(solution)/shard_map/all_gather | solution.py:10
  61.9 10.7 %fusion.3 = f32[2048,1024]{0,1:T(8,128)} fusion(bf16[1024,4096]{1,0:T(8,128)(2,1)} %all-gather.4.cloned.1.call-done, bf16[1024,1024]{1,0:T(8,128)(2,1)} %param.7), kind=kOutput, calls=%fused_computation.8 | convolution fusion | flops 4299161600 | bytes 14680064 | tf_op jit(solution)/shard_map/dot_general | solution.py:49
  72.6 43.1 %all-gather.6.cloned.1.call-done = bf16[2048,1024]{1,0:T(8,128)(2,1)} async-done(((bf16[128,1024]{1,0:T(8,128)(2,1)}), bf16[2048,1024]{1,0:T(8,128)(2,1)}) %all-gather.6.cloned.1.call-update) | async-done | bytes 4194320 | tf_op jit(solution)/shard_map/all_gather | solution.py:34
  115.7 0.0 copy-done.1
  115.7 0.0 copy-start
  115.7 0.0 slice-start
  115.7 8.1 %multiply_convert_fusion.1 = bf16[1024,1024]{1,0:T(8,128)(2,1)S(1)} fusion(bf16[1024,1024]{1,0:T(8,128)(2,1)S(1)} %copy-done.1, bf16[2048,1024]{1,0:T(8,128)(2,1)} %all-gather.6.cloned.1.call-done, bf16[1024,4096]{1,0:T(8,128)(2,1)} %all-gather.4.cloned.1.call-done), kind=kOutput, calls=%fused_computation.5 | convolution fusion | flops 4300210176 | bytes 12582912 | tf_op jit(solution)/shard_map/dot_general | solution.py:32
  123.8 0.0 copy-done
  123.8 0.0 copy-start.2
  123.8 0.0 slice-start.1
  123.9 4.9 %fusion.1 = f32[2048,1024]{0,1:T(8,128)S(1)} fusion(bf16[1024,1024]{1,0:T(8,128)(2,1)S(1)} %multiply_convert_fusion.1, bf16[1024,4096]{1,0:T(8,128)(2,1)S(1)} %copy-done), kind=kOutput, calls=%fused_computation.2 | convolution fusion | flops 4294967296 | bytes 14680064 | tf_op jit(solution)/shard_map/dot_general | solution.py:52
  128.8 0.0 copy-done.2
  128.8 0.0 slice-done
  128.8 0.0 slice-done.1
  128.8 4.8 %fusion = bf16[2048,2048]{0,1:T(8,128)(2,1)} fusion(f32[2048,1024]{0,1:T(8,128)S(1)} %fusion.1, f32[2048,1024]{0,1:T(8,128)S(1)} %bitcast.7), kind=kLoop, calls=%fused_computation.1 | loop fusion | flops 12582912 | bytes 25165824 | tf_op jit(solution)/shard_map/convert_element_type | solution.py:56
  133.6 12.4 %copy.12 = bf16[2048,2048]{1,0:T(8,128)(2,1)} copy(bf16[2048,2048]{0,1:T(8,128)(2,1)} %fusion) | data formatting | bytes 16777216
  146.0 0.0 copy-start.3
  146.0 0.0 reduce-scatter.4.cloned.1.call-update
  146.0 22.9 %all-gather.8.cloned.1.call-done = bf16[2048,1024]{1,0:T(8,128)(2,1)} async-done(((bf16[128,1024]{1,0:T(8,128)(2,1)}), bf16[2048,1024]{1,0:T(8,128)(2,1)}) %all-gather.8.cloned.1.call-update) | async-done | bytes 4194320 | tf_op jit(solution)/shard_map/all_gather | solution.py:40
  169.0 0.0 copy-done.3
  169.0 6.9 %convolution_convert_fusion = bf16[1024,2048]{1,0:T(8,128)(2,1)S(1)} fusion(bf16[1024,1024]{1,0:T(8,128)(2,1)S(1)} %copy-done.3, bf16[2048,1024]{1,0:T(8,128)(2,1)} %all-gather.8.cloned.1.call-done), kind=kOutput, calls=%fused_computation.7 | convolution fusion | flops 4297064448 | bytes 10485760 | tf_op jit(solution)/shard_map/dot_general | solution.py:38
  175.9 53.9 %all_to_all.5 = bf16[8,128,2048]{2,1,0:T(8,128)(2,1)} all-to-all(bf16[8,128,2048]{2,1,0:T(8,128)(2,1)S(1)} %bitcast.8), channel_id=1, replica_groups=mesh['rep'=16,'fs'=4,'tp'=2] {'fs','tp'}, dimensions={0} | all-to-all | bytes 8388608 | tf_op jit(solution)/shard_map/all_to_all | solution.py:22
  229.8 3.9 %reduce_sum.12 = bf16[128,2048]{1,0:T(8,128)(2,1)} reduce(bf16[8,128,2048]{2,1,0:T(8,128)(2,1)} %all_to_all.5, bf16[]{:T(256)} %constant.3.clone.1), dimensions={0}, to_apply=%region_0.0 | reduce | flops 1835008 | bytes 4718594 | tf_op jit(solution)/shard_map/reduce_sum | solution.py:23
  233.6 24.1 %reduce-scatter.4.cloned.1.call-done = bf16[128,2048]{1,0:T(8,128)(2,1)} async-done(((bf16[2048,2048]{1,0:T(8,128)(2,1)}), bf16[128,2048]{1,0:T(8,128)(2,1)}) %reduce-scatter.4.cloned.1.call-update) | async-done | bytes 524304
  257.8 1.3 copy.13
  259.1 0.1 fusion.11
  259.2 1.0 copy.11
  260.2 1.0 copy.10
  (1 shorter events, 0.0 us)
Async XLA Ops:
  7.2 54.7 %all-gather.4.cloned.1.call-start = ((), (), s32[]{:S(2)}) async-start(), calls=%async_computation.2 | async-start | bytes 9437184 | tf_op jit(solution)/shard_map/all_gather | solution.py:10
  9.6 106.1 %all-gather.6.cloned.1.call-start = ((), (), s32[]{:S(2)}) async-start(), calls=%async_computation.3 | async-start | bytes 4456448 | tf_op jit(solution)/shard_map/all_gather | solution.py:34
  10.3 158.6 %all-gather.8.cloned.1.call-start = ((), (), s32[]{:S(2)}) async-start(), calls=%async_computation.4 | async-start | bytes 4456448 | tf_op jit(solution)/shard_map/all_gather | solution.py:40
  11.1 104.6 %copy-start.1 = (bf16[1024,1024]{1,0:T(8,128)(2,1)S(1)}, bf16[1024,1024]{1,0:T(8,128)(2,1)}, u32[]{:S(2)}) copy-start(bf16[1024,1024]{1,0:T(8,128)(2,1)} %param.7) | copy-start | bytes 6291460
  11.1 246.7 %reduce-scatter.4.cloned.1.call-start = ((), (), s32[]{:S(2)}) async-start(), calls=%async_computation.5 | async-start | bytes 8912896
  115.7 8.1 %copy-start = (bf16[1024,4096]{1,0:T(8,128)(2,1)S(1)}, bf16[1024,4096]{1,0:T(8,128)(2,1)}, u32[]{:S(2)}) copy-start(bf16[1024,4096]{1,0:T(8,128)(2,1)} %all-gather.4.cloned.1.call-done) | copy-start | bytes 25165828
  115.7 13.1 %slice-start = ((s8[8388608]{0:T(1024)(128)(4,1)}), s8[4194304]{0:T(1024)(128)(4,1)S(1)}, s32[]{:S(2)}) async-start(s8[8388608]{0:T(1024)(128)(4,1)} %bitcast.6), calls=%async_computation.6 | async-start | bytes 8388608
  123.8 5.0 %copy-start.2 = (bf16[1024,1024]{1,0:T(8,128)(2,1)}, bf16[1024,1024]{1,0:T(8,128)(2,1)S(1)}, u32[]{:S(2)}) copy-start(bf16[1024,1024]{1,0:T(8,128)(2,1)S(1)} %multiply_convert_fusion.1) | copy-start | bytes 6291460
  123.8 5.0 %slice-start.1 = ((s8[8388608]{0:T(1024)(128)(4,1)}), s8[4194304]{0:T(1024)(128)(4,1)S(1)}, s32[]{:S(2)}) async-start(s8[8388608]{0:T(1024)(128)(4,1)} %bitcast.6), calls=%async_computation.7 | async-start | bytes 8388608
  146.0 23.0 %copy-start.3 = (bf16[1024,1024]{1,0:T(8,128)(2,1)S(1)}, bf16[1024,1024]{1,0:T(8,128)(2,1)}, u32[]{:S(2)}) copy-start(bf16[1024,1024]{1,0:T(8,128)(2,1)} %copy-done.2) | copy-start | bytes 6291460
Sparse Core Ops, SparseCore 0:
  9.7 52.1 all-gather.3
  64.0 51.6 all-gather.5
  117.9 51.0 all-gather.7
  172.2 85.5 reduce-scatter.3
where the time goes:
time: 268 us
  waiting for transfers between devices  142 us (53%)
  blocking collectives  53.9 us (20%)
  matrix products  30.7 us (11%)
  local copies, waits for them, and re-layouts  15.8 us (6%)
  between operations  13.9 us (5%)
  other arithmetic  11 us (4%)
    all_to_all x1, blocking collectives, sent_and_summed(): lax.all_to_all(tiles, axis, split_axis=0, concat_axis=0, tiled=True)  53.9 us
    all_gather x1, waiting for transfers between devices, side_by_side(): out = lax.all_gather(both, axis, axis=dim, tiled=True)  50.8 us
    all_gather x1, waiting for transfers between devices, on_device(): lax.all_gather(w_down_t, 'rep', axis=0, tiled=True)  43.1 us
    unnamed x5, waiting for transfers between devices  25.6 us
    all_gather x1, waiting for transfers between devices, on_device(): lax.all_gather(w_up, 'rep', axis=0, tiled=True)  22.9 us
    unnamed x16, local copies, waits for them, and re-layouts  15.7 us
    dot_general x1, matrix products, on_device(): lax.dot_general(grad_rows, squared, (((0,), (0,)), ((), ())), preferred_e...  10.7 us
    dot_general x1, matrix products, on_device(): jnp.dot(grad_rows, lax.all_gather(w_down_t, 'rep', axis=0, tiled=True), p...  8.1 us
  transfers between devices with their start and end apart: 4, of which 4 were waited for; matrix products, arithmetic and copies ran while one was open for 19% of the time, Pallas kernels for 0%

commit v1 on v0

--- a/solution.py
+++ b/solution.py
@@ -2,6 +2,7 @@
 import jax.numpy as jnp
 from jax import lax
 from jax.sharding import PartitionSpec as P
+from jax.lax import axis_index, axis_size, ppermute
 
 
 def side_by_side(arrays, axis, dim, along):
@@ -24,6 +25,34 @@
 
 
 def on_device(inputs, out_grad, pre_act, w_up, w_down_t):
+
+    def zone_check(load, mesh_ax):
+        b_next = axis_size(mesh_ax)
+        mixed_arr, z1, fresh = (b_next, axis_index(mesh_ax), load.shape[0])
+        items = []
+        for tick, i in enumerate(load.shape):
+            items.append(i * mixed_arr if tick == 0 else i)
+        placed = jnp.zeros(items, load.dtype)
+        state_next = lax.dynamic_update_slice_in_dim(placed, load, z1 * fresh, axis=0)
+        wide_out = known = load
+        for b in range(1, mixed_arr // 2 + 1):
+            history = []
+            for tick in range(mixed_arr):
+                history.append((tick, (tick + 1) % mixed_arr))
+            wide_out = ppermute(wide_out, mesh_ax, history)
+            state_next = lax.dynamic_update_slice_in_dim(
+                state_next, wide_out, (z1 - b) % mixed_arr * fresh, axis=0
+            )
+            if 2 * b < mixed_arr:
+                chunks = []
+                for tick in range(mixed_arr):
+                    chunks.append((tick, (tick - 1) % mixed_arr))
+                known = ppermute(known, axis_name=mesh_ax, perm=chunks)
+                state_next = lax.dynamic_update_slice_in_dim(
+                    state_next, known, (z1 + b) % mixed_arr * fresh, axis=0
+                )
+        return state_next
+
     input_rows, grad_rows = side_by_side((inputs, out_grad), ("fs", "tp"), 0, 1)
     row_count, col_count = pre_act.shape
     pre_float = pre_act.astype(jnp.float32)
@@ -37,7 +66,7 @@
     grad_pre = (grad_squared * 2.0 * linear).astype(jnp.bfloat16)
     partial_terms = lax.dot_general(
         grad_pre,
-        lax.all_gather(w_up, "rep", axis=0, tiled=True),
+        zone_check(w_up, "rep"),
         (((1,), (1,)), ((), ())),
         preferred_element_type=jnp.float32,
     ).astype(jnp.bfloat16)

time: 268 us -> 332 us (1.24)
  starting transfers between devices: 0.16 us -> 39.3 us
  local copies, waits for them, and re-layouts: 15.8 us -> 30.8 us
  waiting for transfers between devices: 142 us -> 148 us
    ppermute x0 -> x15, waiting for transfers between devices: none -> 52.3 us  [the longest x8 41.8 us: zone_check(): wide_out = ppermute(wide_out, mesh_ax, history)]
    ppermute x0 -> x15, starting transfers between devices: none -> 39.2 us  [the longest x7 37.7 us: zone_check(): known = ppermute(known, axis_name=mesh_ax, perm=chunks)]
    unnamed x5 -> x4, waiting for transfers between devices: 25.6 us -> 0.73 us
    all_gather x1 -> x0, waiting for transfers between devices: 22.9 us -> none  [on_device(): lax.all_gather(w_up, 'rep', axis=0, tiled=True)]
    dynamic_update_slice x0 -> x16, local copies, waits for them, and re-layouts: none -> 11.6 us  [the longest x8 5.76 us: zone_check(): lax.dynamic_update_slice_in_dim(state_next, wide_out, (z1 - b) % mixed_ar...]
  transfers between devices with their start and end apart: 4 -> 18, of which waited for: 4 -> 14; matrix products, arithmetic and copies ran while one was open for 19% -> 11% of each run, Pallas kernels for 0% -> 0%
where the time goes in v1:
time: 332 us; the launch traced here: 331 us
  waiting for transfers between devices  148 us (45%)
  blocking collectives  56.7 us (17%)
  starting transfers between devices  39.3 us (12%)
  matrix products  31.3 us (9%)
  local copies, waits for them, and re-layouts  30.8 us (9%)
  between operations  13.9 us (4%)
  other arithmetic  11 us (3%)
    all_to_all x1, blocking collectives, sent_and_summed(): lax.all_to_all(tiles, axis, split_axis=0, concat_axis=0, tiled=True)  56.7 us
    all_gather x1, waiting for transfers between devices, side_by_side(): out = lax.all_gather(both, axis, axis=dim, tiled=True)  51.5 us
    all_gather x1, waiting for transfers between devices, on_device(): lax.all_gather(w_down_t, 'rep', axis=0, tiled=True)  43.2 us
    ppermute x8, waiting for transfers between devices, zone_check(): wide_out = ppermute(wide_out, mesh_ax, history)  41.8 us
    ppermute x7, starting transfers between devices, zone_check(): known = ppermute(known, axis_name=mesh_ax, perm=chunks)  37.7 us
    unnamed x16, local copies, waits for them, and re-layouts  16.6 us
    dot_general x1, matrix products, on_device(): lax.dot_general(grad_rows, squared, (((0,), (0,)), ((), ())), preferred_e...  10.6 us
    ppermute x7, waiting for transfers between devices, zone_check(): known = ppermute(known, axis_name=mesh_ax, perm=chunks)  10.5 us
  transfers between devices with their start and end apart: 18, of which 14 were waited for; matrix products, arithmetic and copies ran while one was open for 11% of the time, Pallas kernels for 0%

profile of v1, /device:TPU:0, one launch (start us, length us, event | category | flops | bytes accessed | tf_op | source)
XLA Modules:
  0.0 330.6 jit_solution(11238803849485627972)
XLA Ops:
  7.2 2.4 pad_maximum_fusion
  10.4 51.5 %all-gather.3.cloned.1.call-done = bf16[1024,4096]{1,0:T(8,128)(2,1)} async-done(((bf16[128,4096]{1,0:T(8,128)(2,1)}), bf16[1024,4096]{1,0:T(8,128)(2,1)}) %all-gather.3.cloned.1.call-update) | async-done | bytes 8388624 | tf_op jit(solution)/shard_map/all_gather | solution.py:11
  61.9 10.6 %fusion.3 = f32[2048,1024]{0,1:T(8,128)} fusion(bf16[1024,4096]{1,0:T(8,128)(2,1)} %all-gather.3.cloned.1.call-done, bf16[1024,1024]{1,0:T(8,128)(2,1)} %param.7), kind=kOutput, calls=%fused_computation.8 | convolution fusion | flops 4299161600 | bytes 14680064 | tf_op jit(solution)/shard_map/dot_general | solution.py:78
  72.6 43.2 %all-gather.5.cloned.1.call-done = bf16[2048,1024]{1,0:T(8,128)(2,1)} async-done(((bf16[128,1024]{1,0:T(8,128)(2,1)}), bf16[2048,1024]{1,0:T(8,128)(2,1)}) %all-gather.5.cloned.1.call-update) | async-done | bytes 4194320 | tf_op jit(solution)/shard_map/all_gather | solution.py:63
  115.7 8.7 %multiply_convert_fusion.1 = bf16[1024,1024]{1,0:T(8,128)(2,1)S(1)} fusion(bf16[1024,1024]{1,0:T(8,128)(2,1)} %param.7, bf16[2048,1024]{1,0:T(8,128)(2,1)} %all-gather.5.cloned.1.call-done, bf16[1024,4096]{1,0:T(8,128)(2,1)} %all-gather.3.cloned.1.call-done), kind=kOutput, calls=%fused_computation.5 | convolution fusion | flops 4300210176 | bytes 12582912 | tf_op jit(solution)/shard_map/dot_general | solution.py:61
  124.5 4.9 %fusion.1 = f32[2048,1024]{0,1:T(8,128)S(1)} fusion(bf16[1024,1024]{1,0:T(8,128)(2,1)S(1)} %multiply_convert_fusion.1, bf16[1024,4096]{1,0:T(8,128)(2,1)S(1)} %copy-done.1), kind=kOutput, calls=%fused_computation.2 | convolution fusion | flops 4294967296 | bytes 14680064 | tf_op jit(solution)/shard_map/dot_general | solution.py:81
  129.5 4.8 %fusion = bf16[2048,2048]{0,1:T(8,128)(2,1)} fusion(f32[2048,1024]{0,1:T(8,128)S(1)} %fusion.1, f32[2048,1024]{0,1:T(8,128)S(1)} %bitcast.7), kind=kLoop, calls=%fused_computation.1 | loop fusion | flops 12582912 | bytes 25165824 | tf_op jit(solution)/shard_map/convert_element_type | solution.py:85
  134.2 12.4 %copy.12 = bf16[2048,2048]{1,0:T(8,128)(2,1)} copy(bf16[2048,2048]{0,1:T(8,128)(2,1)} %fusion) | data formatting | bytes 16777216
  146.6 0.9 copy-done
  147.5 1.5 collective-permute-start
  149.0 3.9 %collective-permute-start.1 = (bf16[128,1024]{1,0:T(8,128)(2,1)S(1)}, bf16[128,1024]{1,0:T(8,128)(2,1)S(1)}, u32[]{:S(2)}, u32[]{:S(2)}) collective-permute-start(bf16[128,1024]{1,0:T(8,128)(2,1)S(1)} %copy-done), channel_id=1, source_target_pairs={{0,120},{8,0},{16,8},{24,16},{32,24},{40,32},{48,40},{56,48},{64,5... | collective-permute-start | bytes 786440 | tf_op jit(solution)/shard_map/ppermute | solution.py:50
  152.9 5.9 %collective-permute-done = bf16[128,1024]{1,0:T(8,128)(2,1)S(1)} collective-permute-done((bf16[128,1024]{1,0:T(8,128)(2,1)S(1)}, bf16[128,1024]{1,0:T(8,128)(2,1)S(1)}, u32[]{:S(2)}, u32[]{:S(2)}) %collective-permute-start) | collective-permute-done | bytes 262176 | tf_op jit(solution)/shard_map/ppermute | solution.py:42
  158.7 2.8 collective-permute-done.1
  161.6 5.8 %collective-permute-start.3 = (bf16[128,1024]{1,0:T(8,128)(2,1)S(1)}, bf16[128,1024]{1,0:T(8,128)(2,1)S(1)}, u32[]{:S(2)}, u32[]{:S(2)}) collective-permute-start(bf16[128,1024]{1,0:T(8,128)(2,1)S(1)} %collective-permute-done.1), channel_id=1, source_target_pairs={{0,120},{8,0},{16,8},{24,16},{32,24},{40,32},{48,40},{56,48},{64,5... | collective-permute-start | bytes 786440 | tf_op jit(solution)/shard_map/ppermute | solution.py:50
  167.4 7.9 %collective-permute-done.2 = bf16[128,1024]{1,0:T(8,128)(2,1)S(1)} collective-permute-done((bf16[128,1024]{1,0:T(8,128)(2,1)S(1)}, bf16[128,1024]{1,0:T(8,128)(2,1)S(1)}, u32[]{:S(2)}, u32[]{:S(2)}) %collective-permute-start.2) | collective-permute-done | bytes 262176 | tf_op jit(solution)/shard_map/ppermute | solution.py:42
  175.3 5.3 %collective-permute-start.5 = (bf16[128,1024]{1,0:T(8,128)(2,1)S(1)}, bf16[128,1024]{1,0:T(8,128)(2,1)S(1)}, u32[]{:S(2)}, u32[]{:S(2)}) collective-permute-start(bf16[128,1024]{1,0:T(8,128)(2,1)S(1)} %collective-permute-done.3), channel_id=1, source_target_pairs={{0,120},{8,0},{16,8},{24,16},{32,24},{40,32},{48,40},{56,48},{64,5... | collective-permute-start | bytes 786440 | tf_op jit(solution)/shard_map/ppermute | solution.py:50
  180.7 10.0 %collective-permute-done.4 = bf16[128,1024]{1,0:T(8,128)(2,1)S(1)} collective-permute-done((bf16[128,1024]{1,0:T(8,128)(2,1)S(1)}, bf16[128,1024]{1,0:T(8,128)(2,1)S(1)}, u32[]{:S(2)}, u32[]{:S(2)}) %collective-permute-start.4) | collective-permute-done | bytes 262176 | tf_op jit(solution)/shard_map/ppermute | solution.py:42
  190.7 2.5 broadcast_in_dim.3
  193.2 0.7 constant_dynamic-update-slice_fusion.15
  193.9 0.7 constant_dynamic-update-slice_fusion.14
  194.6 5.3 %collective-permute-start.7 = (bf16[128,1024]{1,0:T(8,128)(2,1)S(1)}, bf16[128,1024]{1,0:T(8,128)(2,1)S(1)}, u32[]{:S(2)}, u32[]{:S(2)}) collective-permute-start(bf16[128,1024]{1,0:T(8,128)(2,1)S(1)} %collective-permute-done.5), channel_id=1, source_target_pairs={{0,120},{8,0},{16,8},{24,16},{32,24},{40,32},{48,40},{56,48},{64,5... | collective-permute-start | bytes 786440 | tf_op jit(solution)/shard_map/ppermute | solution.py:50
  200.0 0.7 constant_dynamic-update-slice_fusion.13
  200.7 5.2 %collective-permute-done.6 = bf16[128,1024]{1,0:T(8,128)(2,1)S(1)} collective-permute-done((bf16[128,1024]{1,0:T(8,128)(2,1)S(1)}, bf16[128,1024]{1,0:T(8,128)(2,1)S(1)}, u32[]{:S(2)}, u32[]{:S(2)}) %collective-permute-start.6) | collective-permute-done | bytes 262176 | tf_op jit(solution)/shard_map/ppermute | solution.py:42
  205.9 0.7 constant_dynamic-update-slice_fusion.12
  206.7 0.7 constant_dynamic-update-slice_fusion.11
  207.4 1.5 collective-permute-done.7
  208.9 5.8 %collective-permute-start.9 = (bf16[128,1024]{1,0:T(8,128)(2,1)S(1)}, bf16[128,1024]{1,0:T(8,128)(2,1)S(1)}, u32[]{:S(2)}, u32[]{:S(2)}) collective-permute-start(bf16[128,1024]{1,0:T(8,128)(2,1)S(1)} %collective-permute-done.7), channel_id=1, source_target_pairs={{0,120},{8,0},{16,8},{24,16},{32,24},{40,32},{48,40},{56,48},{64,5... | collective-permute-start | bytes 786440 | tf_op jit(solution)/shard_map/ppermute | solution.py:50
  215.4 1.8 collective-permute-done.8
  218.0 0.7 constant_dynamic-update-slice_fusion.8
  218.7 5.7 %collective-permute-start.11 = (bf16[128,1024]{1,0:T(8,128)(2,1)S(1)}, bf16[128,1024]{1,0:T(8,128)(2,1)S(1)}, u32[]{:S(2)}, u32[]{:S(2)}) collective-permute-start(bf16[128,1024]{1,0:T(8,128)(2,1)S(1)} %collective-permute-done.9), channel_id=1, source_target_pairs={{0,120},{8,0},{16,8},{24,16},{32,24},{40,32},{48,40},{56,48},{64,5... | collective-permute-start | bytes 786440 | tf_op jit(solution)/shard_map/ppermute | solution.py:50
  224.4 0.7 constant_dynamic-update-slice_fusion.7
  225.1 1.8 collective-permute-done.10
  226.9 0.7 constant_dynamic-update-slice_fusion.6
  227.6 0.7 constant_dynamic-update-slice_fusion.5
  228.4 5.9 %collective-permute-done.11 = bf16[128,1024]{1,0:T(8,128)(2,1)S(1)} collective-permute-done((bf16[128,1024]{1,0:T(8,128)(2,1)S(1)}, bf16[128,1024]{1,0:T(8,128)(2,1)S(1)}, u32[]{:S(2)}, u32[]{:S(2)}) %collective-permute-start.11) | collective-permute-done | bytes 262176 | tf_op jit(solution)/shard_map/ppermute | solution.py:50
  234.3 5.8 %collective-permute-start.13 = (bf16[128,1024]{1,0:T(8,128)(2,1)S(1)}, bf16[128,1024]{1,0:T(8,128)(2,1)S(1)}, u32[]{:S(2)}, u32[]{:S(2)}) collective-permute-start(bf16[128,1024]{1,0:T(8,128)(2,1)S(1)} %collective-permute-done.11), channel_id=1, source_target_pairs={{0,120},{8,0},{16,8},{24,16},{32,24},{40,32},{48,40},{56,48},{64,5... | collective-permute-start | bytes 786440 | tf_op jit(solution)/shard_map/ppermute | solution.py:50
  240.8 1.9 collective-permute-done.12
  242.7 0.7 constant_dynamic-update-slice_fusion.3
  243.4 0.7 constant_dynamic-update-slice_fusion.2
  244.4 0.7 constant_dynamic-update-slice_fusion.1
  245.1 7.3 %collective-permute-done.14 = bf16[128,1024]{1,0:T(8,128)(2,1)S(1)} collective-permute-done((bf16[128,1024]{1,0:T(8,128)(2,1)S(1)}, bf16[128,1024]{1,0:T(8,128)(2,1)S(1)}, u32[]{:S(2)}, u32[]{:S(2)}) %collective-permute-start.14) | collective-permute-done | bytes 262176 | tf_op jit(solution)/shard_map/ppermute | solution.py:42
  252.4 0.7 constant_dynamic-update-slice_fusion
  253.1 7.0 %convolution_convert_fusion = bf16[1024,2048]{1,0:T(8,128)(2,1)S(1)} fusion(bf16[1024,1024]{1,0:T(8,128)(2,1)S(1)} %copy-done.3, bf16[2048,1024]{1,0:T(8,128)(2,1)} %constant_dynamic-update-slice_fusion), kind=kOutput, calls=%fused_computation.7 | convolution fusion | flops 4297064448 | bytes 10485760 | tf_op jit(solution)/shard_map/dot_general | solution.py:67
  260.2 56.7 %all_to_all.5 = bf16[8,128,2048]{2,1,0:T(8,128)(2,1)} all-to-all(bf16[8,128,2048]{2,1,0:T(8,128)(2,1)S(1)} %bitcast.8), channel_id=1, replica_groups=mesh['rep'=16,'fs'=4,'tp'=2] {'fs','tp'}, dimensions={0} | all-to-all | bytes 8388608 | tf_op jit(solution)/shard_map/all_to_all | solution.py:23
  316.9 3.8 %reduce_sum.12 = bf16[128,2048]{1,0:T(8,128)(2,1)} reduce(bf16[8,128,2048]{2,1,0:T(8,128)(2,1)} %all_to_all.5, bf16[]{:T(256)} %constant.97.clone.1), dimensions={0}, to_apply=%region_0.1 | reduce | flops 1835008 | bytes 4718594 | tf_op jit(solution)/shard_map/reduce_sum | solution.py:24
  320.7 1.3 copy.13
  322.1 1.0 copy.11
  323.1 1.0 copy.10
  (34 shorter events, 3.4 us)
Async XLA Ops:
  7.2 54.7 %all-gather.3.cloned.1.call-start = ((), (), s32[]{:S(2)}) async-start(), calls=%async_computation.2 | async-start | bytes 9437184 | tf_op jit(solution)/shard_map/all_gather | solution.py:11
  9.6 106.1 %all-gather.5.cloned.1.call-start = ((), (), s32[]{:S(2)}) async-start(), calls=%async_computation.3 | async-start | bytes 4456448 | tf_op jit(solution)/shard_map/all_gather | solution.py:63
  10.4 310.4 %reduce-scatter.4.cloned.1.call-start = ((), (), s32[]{:S(2)}) async-start(), calls=%async_computation.4 | async-start | bytes 8912896
  115.7 8.7 %copy-start.1 = (bf16[1024,4096]{1,0:T(8,128)(2,1)S(1)}, bf16[1024,4096]{1,0:T(8,128)(2,1)}, u32[]{:S(2)}) copy-start(bf16[1024,4096]{1,0:T(8,128)(2,1)} %all-gather.3.cloned.1.call-done) | copy-start | bytes 25165828
  115.7 13.7 %slice-start = ((s8[8388608]{0:T(1024)(128)(4,1)}), s8[4194304]{0:T(1024)(128)(4,1)S(1)}, s32[]{:S(2)}) async-start(s8[8388608]{0:T(1024)(128)(4,1)} %bitcast.6), calls=%async_computation.5 | async-start | bytes 8388608
  124.4 5.0 %copy-start.2 = (bf16[1024,1024]{1,0:T(8,128)(2,1)}, bf16[1024,1024]{1,0:T(8,128)(2,1)S(1)}, u32[]{:S(2)}) copy-start(bf16[1024,1024]{1,0:T(8,128)(2,1)S(1)} %multiply_convert_fusion.1) | copy-start | bytes 6291460
  124.4 5.0 %slice-start.1 = ((s8[8388608]{0:T(1024)(128)(4,1)}), s8[4194304]{0:T(1024)(128)(4,1)S(1)}, s32[]{:S(2)}) async-start(s8[8388608]{0:T(1024)(128)(4,1)} %bitcast.6), calls=%async_computation.6 | async-start | bytes 8388608
  146.6 0.9 copy-start
  147.5 11.2 %collective-permute-start = (bf16[128,1024]{1,0:T(8,128)(2,1)S(1)}, bf16[128,1024]{1,0:T(8,128)(2,1)S(1)}, u32[]{:S(2)}, u32[]{:S(2)}) collective-permute-start(bf16[128,1024]{1,0:T(8,128)(2,1)S(1)} %copy-done), channel_id=1, source_target_pairs={{0,8},{8,16},{16,24},{24,32},{32,40},{40,48},{48,56},{56,64},{64,7... | collective-permute-start | bytes 786440 | tf_op jit(solution)/shard_map/ppermute | solution.py:42
  149.0 12.6 %collective-permute-start.1 = (bf16[128,1024]{1,0:T(8,128)(2,1)S(1)}, bf16[128,1024]{1,0:T(8,128)(2,1)S(1)}, u32[]{:S(2)}, u32[]{:S(2)}) collective-permute-start(bf16[128,1024]{1,0:T(8,128)(2,1)S(1)} %copy-done), channel_id=1, source_target_pairs={{0,120},{8,0},{16,8},{24,16},{32,24},{40,32},{48,40},{56,48},{64,5... | collective-permute-start | bytes 786440 | tf_op jit(solution)/shard_map/ppermute | solution.py:50
  158.7 16.6 %collective-permute-start.2 = (bf16[128,1024]{1,0:T(8,128)(2,1)S(1)}, bf16[128,1024]{1,0:T(8,128)(2,1)S(1)}, u32[]{:S(2)}, u32[]{:S(2)}) collective-permute-start(bf16[128,1024]{1,0:T(8,128)(2,1)S(1)} %collective-permute-done), channel_id=1, source_target_pairs={{0,8},{8,16},{16,24},{24,32},{32,40},{40,48},{48,56},{56,64},{64,7... | collective-permute-start | bytes 786440 | tf_op jit(solution)/shard_map/ppermute | solution.py:42
  161.6 13.7 %collective-permute-start.3 = (bf16[128,1024]{1,0:T(8,128)(2,1)S(1)}, bf16[128,1024]{1,0:T(8,128)(2,1)S(1)}, u32[]{:S(2)}, u32[]{:S(2)}) collective-permute-start(bf16[128,1024]{1,0:T(8,128)(2,1)S(1)} %collective-permute-done.1), channel_id=1, source_target_pairs={{0,120},{8,0},{16,8},{24,16},{32,24},{40,32},{48,40},{56,48},{64,5... | collective-permute-start | bytes 786440 | tf_op jit(solution)/shard_map/ppermute | solution.py:50
  175.3 15.3 %collective-permute-start.4 = (bf16[128,1024]{1,0:T(8,128)(2,1)S(1)}, bf16[128,1024]{1,0:T(8,128)(2,1)S(1)}, u32[]{:S(2)}, u32[]{:S(2)}) collective-permute-start(bf16[128,1024]{1,0:T(8,128)(2,1)S(1)} %collective-permute-done.2), channel_id=1, source_target_pairs={{0,8},{8,16},{16,24},{24,32},{32,40},{40,48},{48,56},{56,64},{64,7... | collective-permute-start | bytes 786440 | tf_op jit(solution)/shard_map/ppermute | solution.py:42
  175.3 19.3 %collective-permute-start.5 = (bf16[128,1024]{1,0:T(8,128)(2,1)S(1)}, bf16[128,1024]{1,0:T(8,128)(2,1)S(1)}, u32[]{:S(2)}, u32[]{:S(2)}) collective-permute-start(bf16[128,1024]{1,0:T(8,128)(2,1)S(1)} %collective-permute-done.3), channel_id=1, source_target_pairs={{0,120},{8,0},{16,8},{24,16},{32,24},{40,32},{48,40},{56,48},{64,5... | collective-permute-start | bytes 786440 | tf_op jit(solution)/shard_map/ppermute | solution.py:50
  190.7 15.3 %collective-permute-start.6 = (bf16[128,1024]{1,0:T(8,128)(2,1)S(1)}, bf16[128,1024]{1,0:T(8,128)(2,1)S(1)}, u32[]{:S(2)}, u32[]{:S(2)}) collective-permute-start(bf16[128,1024]{1,0:T(8,128)(2,1)S(1)} %collective-permute-done.4), channel_id=1, source_target_pairs={{0,8},{8,16},{16,24},{24,32},{32,40},{40,48},{48,56},{56,64},{64,7... | collective-permute-start | bytes 786440 | tf_op jit(solution)/shard_map/ppermute | solution.py:42
  193.9 59.2 %copy-start.3 = (bf16[1024,1024]{1,0:T(8,128)(2,1)S(1)}, bf16[1024,1024]{1,0:T(8,128)(2,1)}, u32[]{:S(2)}) copy-start(bf16[1024,1024]{1,0:T(8,128)(2,1)} %copy-done.2) | copy-start | bytes 6291460
  194.6 14.3 %collective-permute-start.7 = (bf16[128,1024]{1,0:T(8,128)(2,1)S(1)}, bf16[128,1024]{1,0:T(8,128)(2,1)S(1)}, u32[]{:S(2)}, u32[]{:S(2)}) collective-permute-start(bf16[128,1024]{1,0:T(8,128)(2,1)S(1)} %collective-permute-done.5), channel_id=1, source_target_pairs={{0,120},{8,0},{16,8},{24,16},{32,24},{40,32},{48,40},{56,48},{64,5... | collective-permute-start | bytes 786440 | tf_op jit(solution)/shard_map/ppermute | solution.py:50
  205.9 11.3 %collective-permute-start.8 = (bf16[128,1024]{1,0:T(8,128)(2,1)S(1)}, bf16[128,1024]{1,0:T(8,128)(2,1)S(1)}, u32[]{:S(2)}, u32[]{:S(2)}) collective-permute-start(bf16[128,1024]{1,0:T(8,128)(2,1)S(1)} %collective-permute-done.6), channel_id=1, source_target_pairs={{0,8},{8,16},{16,24},{24,32},{32,40},{40,48},{48,56},{56,64},{64,7... | collective-permute-start | bytes 786440 | tf_op jit(solution)/shard_map/ppermute | solution.py:42
  208.9 9.8 %collective-permute-start.9 = (bf16[128,1024]{1,0:T(8,128)(2,1)S(1)}, bf16[128,1024]{1,0:T(8,128)(2,1)S(1)}, u32[]{:S(2)}, u32[]{:S(2)}) collective-permute-start(bf16[128,1024]{1,0:T(8,128)(2,1)S(1)} %collective-permute-done.7), channel_id=1, source_target_pairs={{0,120},{8,0},{16,8},{24,16},{32,24},{40,32},{48,40},{56,48},{64,5... | collective-permute-start | bytes 786440 | tf_op jit(solution)/shard_map/ppermute | solution.py:50
  217.2 9.7 %collective-permute-start.10 = (bf16[128,1024]{1,0:T(8,128)(2,1)S(1)}, bf16[128,1024]{1,0:T(8,128)(2,1)S(1)}, u32[]{:S(2)}, u32[]{:S(2)}) collective-permute-start(bf16[128,1024]{1,0:T(8,128)(2,1)S(1)} %collective-permute-done.8), channel_id=1, source_target_pairs={{0,8},{8,16},{16,24},{24,32},{32,40},{40,48},{48,56},{56,64},{64,7... | collective-permute-start | bytes 786440 | tf_op jit(solution)/shard_map/ppermute | solution.py:42
  218.7 15.6 %collective-permute-start.11 = (bf16[128,1024]{1,0:T(8,128)(2,1)S(1)}, bf16[128,1024]{1,0:T(8,128)(2,1)S(1)}, u32[]{:S(2)}, u32[]{:S(2)}) collective-permute-start(bf16[128,1024]{1,0:T(8,128)(2,1)S(1)} %collective-permute-done.9), channel_id=1, source_target_pairs={{0,120},{8,0},{16,8},{24,16},{32,24},{40,32},{48,40},{56,48},{64,5... | collective-permute-start | bytes 786440 | tf_op jit(solution)/shard_map/ppermute | solution.py:50
  226.9 15.8 %collective-permute-start.12 = (bf16[128,1024]{1,0:T(8,128)(2,1)S(1)}, bf16[128,1024]{1,0:T(8,128)(2,1)S(1)}, u32[]{:S(2)}, u32[]{:S(2)}) collective-permute-start(bf16[128,1024]{1,0:T(8,128)(2,1)S(1)} %collective-permute-done.10), channel_id=1, source_target_pairs={{0,8},{8,16},{16,24},{24,32},{32,40},{40,48},{48,56},{56,64},{64,7... | collective-permute-start | bytes 786440 | tf_op jit(solution)/shard_map/ppermute | solution.py:42
  234.3 10.1 %collective-permute-start.13 = (bf16[128,1024]{1,0:T(8,128)(2,1)S(1)}, bf16[128,1024]{1,0:T(8,128)(2,1)S(1)}, u32[]{:S(2)}, u32[]{:S(2)}) collective-permute-start(bf16[128,1024]{1,0:T(8,128)(2,1)S(1)} %collective-permute-done.11), channel_id=1, source_target_pairs={{0,120},{8,0},{16,8},{24,16},{32,24},{40,32},{48,40},{56,48},{64,5... | collective-permute-start | bytes 786440 | tf_op jit(solution)/shard_map/ppermute | solution.py:50
  242.7 9.7 %collective-permute-start.14 = (bf16[128,1024]{1,0:T(8,128)(2,1)S(1)}, bf16[128,1024]{1,0:T(8,128)(2,1)S(1)}, u32[]{:S(2)}, u32[]{:S(2)}) collective-permute-start(bf16[128,1024]{1,0:T(8,128)(2,1)S(1)} %collective-permute-done.12), channel_id=1, source_target_pairs={{0,8},{8,16},{16,24},{24,32},{32,40},{40,48},{48,56},{56,64},{64,7... | collective-permute-start | bytes 786440 | tf_op jit(solution)/shard_map/ppermute | solution.py:42
Sparse Core Ops, SparseCore 0:
  9.7 52.1 all-gather.2
  64.0 51.6 all-gather.4
  146.7 99.1 reduce-scatter.3
